TPU v7x, 32 devices: a whole 2x2x4 slice. The times are simulated.
32 devices in a mesh: sp: 8 (over z, y), tp: 4 (over x, core).
Axes of the slice: x: 2, y: 2, z: 4, core: 2. Of those that a mesh axis runs over, the one named last changes fastest.
Arguments:
- tokens: bfloat16 [3072, 2048], P(('sp', 'tp')), may hold values from -6 to 6
- input_norm_gain: bfloat16 [2048], replicated, may hold values from 0.099609375 to 1.8984375
- output_gate_weight: bfloat16 [2048, 2048], P('sp', 'tp'), may hold values from -0.125 to 0.125
- value_input_weight: bfloat16 [2048, 2048], P('sp', 'tp'), may hold values from -0.125 to 0.125
- recurrence_input_weight: bfloat16 [2048, 2048], P('sp', 'tp'), may hold values from -0.125 to 0.125
- convolution_filter: bfloat16 [3, 2048], P(None, 'tp'), may hold values from -3.5 to 3.5
- recurrence_filter: bfloat16 [4, 2048], P(None, 'tp'), may hold values from -3 to 3
- recurrence_gate_matrix: bfloat16 [8, 256, 256], P('tp'), may hold values from -0.375 to 0.375
- input_gate_matrix: bfloat16 [8, 256, 256], P('tp'), may hold values from -0.375 to 0.375
- channel_decay_rate: float32 [2048], P('tp'), may hold values from 1.6276042e-05 to 0.025
- head_log_decay_add: float32 [8, 3072], P('tp', 'sp'), may hold values from -0.7 to 0
- initial_state: float32 [2048], P('tp'), may hold values from -6 to 6
- output_matrix: bfloat16 [2048, 2048], P(None, 'tp'), may hold values from -0.125 to 0.125
Outputs:
- mixed: bfloat16 [3072, 2048], P(('sp', 'tp'))
All inputs are finite; a program needn't handle non-finite values.
Results may differ from a plain program's by a relative error of at most 0.015.
Values may be sent and summed in bfloat16 or wider, within the bound.
A program may use at most 64 MiB of HBM per device.

v0:
```python
import jax
import jax.numpy as jnp
from jax import lax
from jax.sharding import PartitionSpec as P

DECAY_MULTIPLIER = 8.0
NORM_EPS = 1e-06


def shifted(value, axis, steps):
    count = lax.axis_size(axis)
    first, last = (max(0, -steps), min(count, count - steps))
    return lax.ppermute(value, axis, [(source, source + steps) for source in range(first, last)])


def causal_taps(values, before, tap_weights):
    extended = jnp.concatenate([before, values], axis=0).astype(jnp.float32)
    length = values.shape[0]
    summed = jnp.zeros((length, values.shape[1]), jnp.float32)
    for offset in range(tap_weights.shape[0]):
        summed = (
            summed + tap_weights[offset].astype(jnp.float32) * extended[offset : offset + length]
        )
    return summed


def linear_step(first_pair, second_pair):
    return (first_pair[0] * second_pair[0], second_pair[0] * first_pair[1] + second_pair[1])


def shards(
    tokens,
    input_norm_gain,
    output_gate_weight,
    value_input_weight,
    recurrence_input_weight,
    convolution_filter,
    recurrence_filter,
    recurrence_gate_matrix,
    input_gate_matrix,
    channel_decay_rate,
    head_log_decay_add,
    initial_state,
    output_matrix,
):
    token_rows = tokens.astype(jnp.float32)
    inverse_rms = lax.rsqrt(jnp.mean(token_rows * token_rows, axis=1, keepdims=True) + NORM_EPS)
    normed = (token_rows * inverse_rms * input_norm_gain.astype(jnp.float32)).astype(jnp.bfloat16)
    channel_count = output_gate_weight.shape[1]
    weights = (
        lax.all_gather(output_gate_weight, "sp", axis=0, tiled=True),
        lax.all_gather(value_input_weight, "sp", axis=0, tiled=True),
        lax.all_gather(recurrence_input_weight, "sp", axis=0, tiled=True),
    )
    row_block = lax.all_gather(normed, "tp", axis=0, tiled=True)
    projected = jnp.concatenate(
        [
            jnp.dot(row_block, weight, preferred_element_type=jnp.float32).astype(jnp.bfloat16)
            for weight in weights
        ],
        axis=1,
    )
    gate_proj = projected[:, :channel_count]
    value_proj = projected[:, channel_count : 2 * channel_count]
    recur_proj = projected[:, 2 * channel_count :]
    value_tail, recur_tail = shifted(
        (
            value_proj[-(convolution_filter.shape[0] - 1) :],
            recur_proj[-(recurrence_filter.shape[0] - 1) :],
        ),
        "sp",
        1,
    )
    conv_mix = gate_proj.astype(jnp.float32) * causal_taps(
        value_proj, value_tail, convolution_filter
    )
    recur_in = causal_taps(recur_proj, recur_tail, recurrence_filter).astype(jnp.bfloat16)
    length = recur_in.shape[0]
    number_of_heads = recurrence_gate_matrix.shape[0]
    head_width = channel_count // number_of_heads
    grouped = recur_in.reshape(length, number_of_heads, head_width)
    forget_gate = jax.nn.sigmoid(
        jnp.einsum(
            "thi,hij->thj", grouped, recurrence_gate_matrix, preferred_element_type=jnp.float32
        ).reshape(length, channel_count)
    )
    admit_gate = jax.nn.sigmoid(
        jnp.einsum(
            "thi,hij->thj", grouped, input_gate_matrix, preferred_element_type=jnp.float32
        ).reshape(length, channel_count)
    )
    decay_add_rows = jnp.repeat(head_log_decay_add.T, head_width, axis=1)
    logarithm_decay = -DECAY_MULTIPLIER * forget_gate * channel_decay_rate[None, :] + decay_add_rows
    decay_step = jnp.exp(logarithm_decay)
    drive_term = (
        recur_in.astype(jnp.float32) * admit_gate * jnp.sqrt(-jnp.expm1(2.0 * logarithm_decay))
    )
    cum_decay, local_state = lax.associative_scan(linear_step, (decay_step, drive_term), axis=0)
    block_log = jnp.sum(logarithm_decay, axis=0)
    block_end = local_state[-1]
    all_logs, all_ends = (
        lax.all_gather(block_log[None, :], "sp", axis=0, tiled=True),
        lax.all_gather(block_end[None, :], "sp", axis=0, tiled=True),
    )
    devices = all_logs.shape[0]
    position = lax.axis_index("sp")
    earlier = (jnp.arange(devices, dtype=jnp.int32) < position)[:, None]
    masked_logs = jnp.where(earlier, all_logs, 0.0)
    through = jnp.cumsum(masked_logs, axis=0)
    prior_log = jnp.sum(masked_logs, axis=0)
    weights_back = jnp.where(earlier, jnp.exp(jnp.minimum(prior_log[None, :] - through, 0.0)), 0.0)
    incoming = jnp.exp(prior_log) * initial_state + jnp.sum(weights_back * all_ends, axis=0)
    hidden = local_state + cum_decay * incoming[None, :]
    merged = (conv_mix + hidden).astype(jnp.bfloat16)
    contract = (((1,), (1,)), ((), ()))
    return lax.psum_scatter(
        lax.dot_general(merged, output_matrix, contract, preferred_element_type=jnp.float32).astype(
            jnp.bfloat16
        ),
        "tp",
        scatter_dimension=0,
        tiled=True,
    )


def solution(mesh):
    placed = (
        P(("sp", "tp"), None),
        P(),
        P("sp", "tp"),
        P("sp", "tp"),
        P("sp", "tp"),
        P(None, "tp"),
        P(None, "tp"),
        P("tp", None, None),
        P("tp", None, None),
        P("tp"),
        P("tp", "sp"),
        P("tp"),
        P(None, "tp"),
    )
    return jax.shard_map(
        shards, mesh=mesh, in_specs=placed, out_specs=P(("sp", "tp"), None), check_vma=False
    )
```

profile of v0, /device:TPU:5, one launch (start us, length us, event | category | flops | bytes accessed | tf_op | source)
XLA Modules:
  0.0 280.2 jit_solution(6480056698027380360)
XLA Ops:
  8.6 1.9 fusion.12
  14.0 17.9 %all-gather.7.cloned.1.call-done = bf16[384,2048]{1,0:T(8,128)(2,1)} async-done(((bf16[96,2048]{1,0:T(8,128)(2,1)}), bf16[384,2048]{1,0:T(8,128)(2,1)}) %all-gather.7.cloned.1.call-update) | async-done | bytes 1572880 | tf_op jit(solution)/shard_map/all_gather | solution.py:55
  31.9 48.0 %all-gather.11.cloned.1.call-done = bf16[2048,512]{1,0:T(8,128)(2,1)} async-done(((bf16[256,512]{1,0:T(8,128)(2,1)}), bf16[2048,512]{1,0:T(8,128)(2,1)}) %all-gather.11.cloned.1.call-update) | async-done | bytes 2097168 | tf_op jit(solution)/shard_map/all_gather | solution.py:52
  80.0 3.0 %convolution_convert_fusion.2 = bf16[384,512]{1,0:T(8,128)(2,1)S(1)} fusion(bf16[384,2048]{1,0:T(8,128)(2,1)} %all-gather.7.cloned.1.call-done, bf16[2048,512]{1,0:T(8,128)(2,1)} %all-gather.11.cloned.1.call-done), kind=kOutput, calls=%fused_computation.10 | convolution fusion | flops 805502976 | bytes 4063232 | tf_op jit(solution)/shard_map/dot_general | solution.py:58
  83.0 4.9 %collective-permute-start = (bf16[2,512]{1,0:T(2,128)(2,1)S(1)}, bf16[2,512]{1,0:T(2,128)(2,1)S(1)}, u32[]{:S(2)}, u32[]{:S(2)}) collective-permute-start(bf16[2,512]{1,0:T(2,128)(2,1)S(1)} %slice.380), channel_id=1, source_target_pairs={{0,4},{4,8},{8,12},{12,16},{16,20},{20,24},{24,28},{1,5},{5,9},{9,... | collective-permute-start | bytes 6152 | tf_op jit(solution)/shard_map/ppermute | solution.py:13
  87.9 41.8 %all-gather.13.cloned.1.call-done = bf16[2048,512]{1,0:T(8,128)(2,1)} async-done(((bf16[256,512]{1,0:T(8,128)(2,1)}), bf16[2048,512]{1,0:T(8,128)(2,1)}) %all-gather.13.cloned.1.call-update) | async-done | bytes 2097168 | tf_op jit(solution)/shard_map/all_gather | solution.py:53
  129.7 3.0 %convolution_convert_fusion.1 = bf16[384,512]{1,0:T(8,128)(2,1)S(1)} fusion(bf16[384,2048]{1,0:T(8,128)(2,1)} %all-gather.7.cloned.1.call-done, bf16[2048,512]{1,0:T(8,128)(2,1)} %all-gather.13.cloned.1.call-done), kind=kOutput, calls=%fused_computation.9 | convolution fusion | flops 805502976 | bytes 4063232 | tf_op jit(solution)/shard_map/dot_general | solution.py:58
  132.8 4.9 %collective-permute-start.1 = (bf16[3,512]{1,0:T(4,128)(2,1)S(1)}, bf16[3,512]{1,0:T(4,128)(2,1)S(1)}, u32[]{:S(2)}, u32[]{:S(2)}) collective-permute-start(bf16[3,512]{1,0:T(4,128)(2,1)S(1)} %slice.384), channel_id=1, source_target_pairs={{0,4},{4,8},{8,12},{12,16},{16,20},{20,24},{24,28},{1,5},{5,9},{9,... | collective-permute-start | bytes 9224 | tf_op jit(solution)/shard_map/ppermute | solution.py:13
  141.0 2.3 copy.30
  143.3 2.3 fusion.22
  145.6 2.3 copy.31
  147.9 3.4 %sqrt_multiply_fusion = (f32[384,512]{1,0:T(8,128)S(1)}, f32[384,512]{1,0:T(8,128)}) fusion(f32[384,512]{1,0:T(8,128)} %copy.30, f32[384,512]{1,0:T(8,128)} %copy.32, f32[384,512]{1,0:T(8,128)} %copy.31, f32[512]{0:T(512)S(1)} %broadcast_multiply_fusion, f32[387,512]{1,0:T(8,128)S(1)} %maximum_convert_fusion.1, f32[512]{0:T(512)S(1)} %bitcast.56, ...), kind=kLoop, calls=%fused_computation.41 | loop fusion | flops 2949120 | bytes 7088128 | tf_op jit(solution)/shard_map/mul | solution.py:96
  152.3 3.2 %slice.363 = f32[191,512]{1,0:T(8,128)} slice(f32[384,512]{1,0:T(8,128)} %copy-done.2), slice={[2:384:2], [0:512:1]} | slice | bytes 782336 | tf_op jit(solution)/shard_map/slice | solution.py:98
  155.4 2.1 slice.307
  157.5 3.2 %slice.306 = f32[192,512]{1,0:T(8,128)} slice(f32[384,512]{1,0:T(8,128)} %copy-done.2), slice={[0:383:2], [0:512:1]} | slice | bytes 786432 | tf_op jit(solution)/shard_map/slice | solution.py:98
  170.1 20.2 %all-gather = f32[8,1,512]{2,1,0:T(1,128)S(1)} all-gather(f32[1,1,512]{2,1,0:T(1,128)S(1)} %reshape.51), channel_id=1, replica_groups=mesh['sp'=8,'tp'=4] {'sp'}, dimensions={0}, use_global_device_ids=true | all-gather | bytes 18432 | tf_op jit(solution)/shard_map/all_gather | solution.py:102
  194.2 2.5 pad.127
  196.7 1.9 add.261
  200.5 1.9 pad.112
  202.4 2.9 %pad.113 = f32[384,512]{1,0:T(8,128)} pad(f32[192,512]{1,0:T(8,128)} %add.252, f32[]{:T(128)} %constant.8.clone.1), padding=1_0_1x0_0_0 | pad | bytes 1179652 | tf_op jit(solution)/shard_map/pad | solution.py:98
  205.3 2.0 pad.128
  208.1 20.5 %all-gather.1 = f32[8,1,512]{2,1,0:T(1,128)S(1)} all-gather(f32[1,1,512]{2,1,0:T(1,128)S(1)} %add_bitcast_fusion), channel_id=1, replica_groups=mesh['sp'=8,'tp'=4] {'sp'}, dimensions={0}, use_global_device_ids=true | all-gather | bytes 18432 | tf_op jit(solution)/shard_map/all_gather | solution.py:103
  228.8 6.7 %convolution_convert_fusion = bf16[384,2048]{1,0:T(8,128)(2,1)} fusion(bf16[2048,512]{1,0:T(8,128)(2,1)S(1)} %copy-done, bf16[384,2048]{1,0:T(8,128)(2,1)} %all-gather.7.cloned.1.call-done, bf16[2048,512]{1,0:T(8,128)(2,1)} %all-gather.9.cloned.1.call-done, f32[386,512]{1,0:T(8,128)} %maximum_convert_fusion, f32[384,512]{1,0:T(8,128)} %pad.128, ...), kind=kOutput, calls=%fused_computation | convolution fusion | flops 1614151680 | bytes 12853248 | tf_op jit(solution)/shard_map/dot_general | solution.py:117
  235.5 38.2 %reduce-scatter.2.cloned.1.call-done = bf16[96,2048]{1,0:T(8,128)(2,1)} async-done(((bf16[384,2048]{1,0:T(8,128)(2,1)}), bf16[96,2048]{1,0:T(8,128)(2,1)}) %reduce-scatter.2.cloned.1.call-update) | async-done | bytes 393232 | tf_op jit(solution)/shard_map/reduce_scatter | solution.py:116
  (184 shorter events, 25.2 us)
Async XLA Ops:
  6.5 222.3 %copy-start = (bf16[2048,512]{1,0:T(8,128)(2,1)S(1)}, bf16[2048,512]{1,0:T(8,128)(2,1)}, u32[]{:S(2)}) copy-start(bf16[2048,512]{1,0:T(8,128)(2,1)} %param.25) | copy-start | bytes 6291460
  6.5 6.1 %copy-start.11 = (f32[512]{0:T(512)S(1)}, f32[512]{0:T(512)}, u32[]{:S(2)}) copy-start(f32[512]{0:T(512)} %param.22) | copy-start | bytes 6148
  6.5 6.2 %copy-start.9 = (bf16[3,512]{1,0:T(4,128)(2,1)S(1)}, bf16[3,512]{1,0:T(4,128)(2,1)}, u32[]{:S(2)}) copy-start(bf16[3,512]{1,0:T(4,128)(2,1)} %param.18) | copy-start | bytes 9220
  6.5 6.2 %copy-start.8 = (bf16[4,512]{1,0:T(4,128)(2,1)S(1)}, bf16[4,512]{1,0:T(4,128)(2,1)}, u32[]{:S(2)}) copy-start(bf16[4,512]{1,0:T(4,128)(2,1)} %param.19) | copy-start | bytes 12292
  6.5 6.2 %copy-start.10 = (f32[2,384]{1,0:T(2,128)S(1)}, f32[2,384]{1,0:T(2,128)}, u32[]{:S(2)}) copy-start(f32[2,384]{1,0:T(2,128)} %param.23) | copy-start | bytes 9220
  6.5 25.4 %all-gather.7.cloned.1.call-start = ((), (), s32[]{:S(2)}) async-start(), calls=%async_computation.1 | async-start | bytes 1966080 | tf_op jit(solution)/shard_map/all_gather | solution.py:55
  10.5 69.4 %all-gather.11.cloned.1.call-start = ((), (), s32[]{:S(2)}) async-start(), calls=%async_computation.3 | async-start | bytes 2359296 | tf_op jit(solution)/shard_map/all_gather | solution.py:52
  11.3 118.4 %all-gather.13.cloned.1.call-start = ((), (), s32[]{:S(2)}) async-start(), calls=%async_computation.4 | async-start | bytes 2359296 | tf_op jit(solution)/shard_map/all_gather | solution.py:53
  12.0 216.7 %all-gather.9.cloned.1.call-start = ((), (), s32[]{:S(2)}) async-start(), calls=%async_computation.2 | async-start | bytes 2359296 | tf_op jit(solution)/shard_map/all_gather | solution.py:51
  12.6 261.1 %reduce-scatter.2.cloned.1.call-start = ((), (), s32[]{:S(2)}) async-start(), calls=%async_computation.5 | async-start | bytes 1966080 | tf_op jit(solution)/shard_map/reduce_scatter | solution.py:116
  83.0 54.7 %collective-permute-start = (bf16[2,512]{1,0:T(2,128)(2,1)S(1)}, bf16[2,512]{1,0:T(2,128)(2,1)S(1)}, u32[]{:S(2)}, u32[]{:S(2)}) collective-permute-start(bf16[2,512]{1,0:T(2,128)(2,1)S(1)} %slice.380), channel_id=1, source_target_pairs={{0,4},{4,8},{8,12},{12,16},{16,20},{20,24},{24,28},{1,5},{5,9},{9,... | collective-permute-start | bytes 6152 | tf_op jit(solution)/shard_map/ppermute | solution.py:13
  132.8 5.9 %collective-permute-start.1 = (bf16[3,512]{1,0:T(4,128)(2,1)S(1)}, bf16[3,512]{1,0:T(4,128)(2,1)S(1)}, u32[]{:S(2)}, u32[]{:S(2)}) collective-permute-start(bf16[3,512]{1,0:T(4,128)(2,1)S(1)} %slice.384), channel_id=1, source_target_pairs={{0,4},{4,8},{8,12},{12,16},{16,20},{20,24},{24,28},{1,5},{5,9},{9,... | collective-permute-start | bytes 9224 | tf_op jit(solution)/shard_map/ppermute | solution.py:13
  138.7 0.9 copy-start.13
  151.4 0.9 copy-start.2
  151.4 9.3 %copy-start.1 = (f32[384,512]{1,0:T(8,128)S(1)}, f32[384,512]{1,0:T(8,128)}, u32[]{:S(2)}) copy-start(f32[384,512]{1,0:T(8,128)} %get-tuple-element.12) | copy-start | bytes 2359300
  196.7 2.7 copy-start.3
  196.7 2.7 copy-start.4
  196.7 2.7 copy-start.5
  200.4 4.9 %copy-start.6 = (f32[191,512]{1,0:T(8,128)S(1)}, f32[191,512]{1,0:T(8,128)}, u32[]{:S(2)}) copy-start(f32[191,512]{1,0:T(8,128)} %get-tuple-element.14) | copy-start | bytes 1173508
  200.5 6.8 %copy-start.7 = (f32[192,512]{1,0:T(8,128)S(1)}, f32[192,512]{1,0:T(8,128)}, u32[]{:S(2)}) copy-start(f32[192,512]{1,0:T(8,128)} %add.261) | copy-start | bytes 1179652
  202.4 26.4 %copy-start.12 = (f32[512]{0:T(512)S(1)}, f32[512]{0:T(512)}, u32[]{:S(2)}) copy-start(f32[512]{0:T(512)} %param.24) | copy-start | bytes 6148
Sparse Core Ops, SparseCore 0:
  10.7 21.2 all-gather.6
  34.0 45.8 all-gather.10
  82.1 47.6 all-gather.12
  131.7 47.7 all-gather.8
  235.7 38.0 reduce-scatter.1
where the time goes:
time: 283 us; the launch traced here: 280 us
  waiting for transfers between devices  148 us (52%)
  blocking collectives  40.8 us (14%)
  local copies, waits for them, and re-layouts  33.3 us (12%)
  other arithmetic  17.9 us (6%)
  matrix products  16.4 us (6%)
  between operations  14 us (5%)
  starting transfers between devices  10 us (4%)
    all_gather x1, waiting for transfers between devices, shards(): lax.all_gather(value_input_weight, 'sp', axis=0, tiled=True)  48 us
    all_gather x1, waiting for transfers between devices, shards(): lax.all_gather(recurrence_input_weight, 'sp', axis=0, tiled=True)  41.8 us
    reduce_scatter x1, waiting for transfers between devices, shards(): lax.psum_scatter(lax.dot_general(merged, output_matrix, contract, preferr...  38.2 us
    all_gather x1, blocking collectives, shards(): lax.all_gather(block_end[None, :], 'sp', axis=0, tiled=True)  20.5 us
    all_gather x1, blocking collectives, shards(): lax.all_gather(block_log[None, :], 'sp', axis=0, tiled=True)  20.2 us
    all_gather x1, waiting for transfers between devices, shards(): row_block = lax.all_gather(normed, 'tp', axis=0, tiled=True)  17.9 us
    slice x56, local copies, waits for them, and re-layouts, shards(): lax.associative_scan(linear_step, (decay_step, drive_term), axis=0)  15.2 us
    pad x30, local copies, waits for them, and re-layouts, shards(): lax.associative_scan(linear_step, (decay_step, drive_term), axis=0)  10.8 us
  transfers between devices with their start and end apart: 7, of which 4 were waited for; matrix products, arithmetic and copies ran while one was open for 20% of the time, Pallas kernels for 0%

commit v1 on v0

v1 whole, which is shorter than its diff:
```python
import functools

import jax
import jax.numpy as jnp
from jax import lax
from jax.experimental import pallas as pl
from jax.experimental.pallas import tpu as pltpu
from jax.sharding import PartitionSpec as P

DECAY_MULTIPLIER = 8.0
NORM_EPS = 1e-06
MESH = pl.DeviceIdType.MESH
HALO = 16
F32 = jnp.float32
BF16 = jnp.bfloat16


def remote(src, dst, send_sem, recv_sem, where):
    return pltpu.make_async_remote_copy(
        src_ref=src,
        dst_ref=dst,
        send_sem=send_sem,
        recv_sem=recv_sem,
        device_id=where,
        device_id_type=MESH,
    )


def one_minus_exp(x, exp_x):
    series = 1.0 + x * (1.0 / 8.0)
    for order in (7.0, 6.0, 5.0, 4.0, 3.0, 2.0):
        series = 1.0 + x * (1.0 / order) * series
    return jnp.where(x > -0.5, -x * series, 1.0 - exp_x)


def kernel(
    n_sp, n_tp, fast, inner,
    tok_ref, gain_ref, gate_ref, value_ref, recur_ref, cf_ref, rf_ref, gr_ref, gi_ref,
    rate_ref, hl_ref, init_ref, wo_ref,
    out_ref,
    tokx, nrm, wgt, wos, acc, us, cm, hs, ca_s, hlb, ex, mg, mgx, oacc,
    loc_sem, w_recv, up_send, dn_send, y_send,
    tk_recv, tk_send, tk_fwd, wo_recv, wo_send, wo_fwd,
    halo_sem, x_send, x_recv, m_send, m_recv,
):
    s, t = lax.axis_index("sp"), lax.axis_index("tp")
    slow, outer = n_sp // fast, n_tp // inner
    z, y = lax.div(s, fast), lax.rem(s, fast)
    o, i = lax.div(t, inner), lax.rem(t, inner)
    rows = tok_ref.shape[0]
    block = rows * n_tp
    chans = gate_ref.shape[1]
    kz = nrm.shape[2]

    def tok_at(q):
        return tokx.at[pl.ds(pl.multiple_of(HALO + q * rows, 16), rows)]

    local = [
        pltpu.make_async_copy(ref, wgt.at[p, s], loc_sem.at[p])
        for p, ref in enumerate((gate_ref, value_ref, recur_ref))
    ]
    local.append(pltpu.make_async_copy(tok_ref, tok_at(t), loc_sem.at[3]))
    local.append(pltpu.make_async_copy(wo_ref, wos.at[t], loc_sem.at[4]))
    for copy in local:
        copy.start()

    barrier = pltpu.get_barrier_semaphore()

    def greet_sp(d, c):
        pl.semaphore_signal(barrier, inc=1, device_id=(lax.rem(s + d, n_sp), t), device_id_type=MESH)
        return c

    def greet_tp(d, c):
        pl.semaphore_signal(barrier, inc=1, device_id=(s, lax.rem(t + d, n_tp)), device_id_type=MESH)
        return c

    lax.fori_loop(1, n_sp, greet_sp, 0)
    lax.fori_loop(1, n_tp, greet_tp, 0)
    for copy in local[:4]:
        copy.wait()
    pl.semaphore_wait(barrier, n_sp + n_tp - 2)

    def slab(q):
        return wgt.at[:, q]

    def up(q):
        return remote(slab(q), slab(q), up_send.at[q], w_recv.at[q], (lax.min(s + fast, n_sp - 1), t))

    def down(q):
        return remote(slab(q), slab(q), dn_send.at[q], w_recv.at[q], (lax.max(s - fast, 0), t))

    def across(q, d):
        return remote(
            slab(q), slab(q), y_send.at[q, d - 1], w_recv.at[q], (z * fast + lax.rem(y + d, fast), t)
        )

    def arrived(q):
        across(q, 1).wait_recv()

    def send_across(q):
        for d in range(1, fast):
            across(q, d).start()

    has_up, has_down = z + 1 < slow, z >= 1

    @pl.when(has_up)
    def _():
        up(s).start()

    @pl.when(has_down)
    def _():
        down(s).start()

    send_across(s)

    def at(oo, ii):
        return oo * inner + ii

    def straight(view, q, ssem, rsem, d):
        return remote(view(q), view(q), ssem.at[d - 1], rsem.at[q], (s, at(lax.rem(o + d, outer), i)))

    def inside(view, q, ssem, rsem, d, oo):
        return remote(view(q), view(q), ssem.at[oo, d - 1], rsem.at[q], (s, at(o, lax.rem(i + d, inner))))

    def wo_at(q):
        return wos.at[q]

    def spread(view, ssem, fsem, rsem):
        for d in range(1, outer):
            straight(view, t, ssem, rsem, d).start()
        for d in range(1, inner):
            inside(view, t, fsem, rsem, d, 0).start()

    def pass_on(view, fsem, rsem, ssem):
        for d in range(1, outer):
            q = at(lax.rem(o + d, outer), i)
            straight(view, q, ssem, rsem, d).wait_recv()
            for e in range(1, inner):
                inside(view, q, fsem, rsem, e, d).start()

    def rest(view, fsem, rsem):
        for d in range(0, outer):
            for e in range(1, inner):
                q = at(lax.rem(o + d, outer), lax.rem(i + e, inner))
                inside(view, q, fsem, rsem, e, d).wait_recv()

    def sent(view, ssem, fsem, rsem):
        for d in range(1, outer):
            straight(view, t, ssem, rsem, d).wait_send()
        for d in range(0, outer):
            for e in range(1, inner):
                q = at(lax.rem(o + d, outer), i)
                inside(view, q, fsem, rsem, e, d).wait_send()

    spread(tok_at, tk_send, tk_fwd, tk_recv)
    local[4].wait()
    spread(wo_at, wo_send, wo_fwd, wo_recv)

    lanes = hlb.shape[2]
    for h in range(hl_ref.shape[0]):
        hlb[h] = jnp.broadcast_to(hl_ref[h : h + 1, :], (lanes, block)).T

    pass_on(tok_at, tk_fwd, tk_recv, tk_send)
    rest(tok_at, tk_fwd, tk_recv)

    halo = remote(
        tokx.at[pl.ds(block, HALO)], tokx.at[pl.ds(0, HALO)],
        halo_sem.at[0], halo_sem.at[1], (lax.min(s + 1, n_sp - 1), t),
    )

    @pl.when(s + 1 < n_sp)
    def _():
        halo.start()

    def normalize(r0):
        x = tokx[pl.ds(r0, HALO), :].astype(F32)
        inv = lax.rsqrt(jnp.mean(x * x, axis=1, keepdims=True) + NORM_EPS)
        n = (x * inv * gain_ref[...].astype(F32)).astype(BF16)
        for b in range(slow):
            nrm[b, pl.ds(r0, HALO), :] = n[:, b * kz : (b + 1) * kz]

    def norm_step(r, c):
        normalize(pl.multiple_of(r * HALO, HALO))
        return c

    lax.fori_loop(1, block // HALO + 1, norm_step, 0)

    @pl.when(s == 0)
    def _():
        tokx[pl.ds(0, HALO), :] = jnp.zeros((HALO, tokx.shape[1]), BF16)

    @pl.when(s > 0)
    def _():
        halo.wait_recv()

    normalize(0)

    def multiply(b, first):
        for d in range(1, fast):
            arrived(b * fast + lax.rem(y + d, fast))

        def step(p, c):
            w = wgt[p, pl.ds(b * fast, fast)].reshape(kz, chans)
            part = jnp.dot(nrm[b], w, preferred_element_type=F32)
            if first:
                acc[p] = part
            else:
                acc[p] = acc[p] + part
            return c

        lax.fori_loop(0, 3, step, 0)

    def multiply_step(k):
        if k == 0:
            multiply(z, True)
            return

        @pl.when(z >= k)
        def _():
            multiply(z - k, False)

        @pl.when(z + k < slow)
        def _():
            multiply(z + k, False)

    for k in range(1, slow):
        @pl.when(z >= k)
        def _():
            q = s - k * fast
            arrived(q)

            @pl.when(has_up)
            def _():
                up(q).start()

            send_across(q)

        @pl.when(z + k < slow)
        def _():
            q = s + k * fast
            arrived(q)

            @pl.when(has_down)
            def _():
                down(q).start()

            send_across(q)

        multiply_step(k - 1)
    multiply_step(slow - 1)

    pass_on(wo_at, wo_fwd, wo_recv, wo_send)

    size = 32
    v_taps, r_taps = cf_ref.shape[0], rf_ref.shape[0]

    def conv_step(j, c):
        r0 = pl.multiple_of(j * size, size)

        def window(p):
            return acc[p, pl.ds(pl.multiple_of(r0 + HALO - 8, 8), size + 8), :].astype(BF16).astype(F32)

        def taps(x, ref):
            n = ref.shape[0]
            first = 8 - (n - 1)
            total = ref[0:1, :].astype(F32) * x[first : first + size]
            for k in range(1, n):
                total = total + ref[k : k + 1, :].astype(F32) * x[first + k : first + k + size]
            return total

        us[pl.ds(r0, size), :] = taps(window(2), rf_ref).astype(BF16)
        cm[pl.ds(r0, size), :] = window(0)[8:] * taps(window(1), cf_ref)
        return c

    lax.fori_loop(0, block // size, conv_step, 0)

    heads, width = gr_ref.shape[0], gr_ref.shape[1]
    for h in range(heads):
        cols = pl.ds(h * width, width)
        u = us[:, cols]
        acc[0, pl.ds(0, block), cols] = jnp.dot(u, gr_ref[h], preferred_element_type=F32)
        acc[1, pl.ds(0, block), cols] = jnp.dot(u, gi_ref[h], preferred_element_type=F32)

    row_id = lax.broadcasted_iota(jnp.int32, (size, chans), 0)

    def scan_step(j, carry):
        carry_a, carry_b = carry
        r0 = pl.multiple_of(j * size, size)
        here = pl.ds(r0, size)
        forget = 1.0 / (1.0 + jnp.exp(-acc[0, here, :]))
        admit = 1.0 / (1.0 + jnp.exp(-acc[1, here, :]))
        add = jnp.concatenate(
            [hlb[h, here, :] for h in range(heads) for _ in range(width // lanes)], axis=1
        )
        log_decay = -DECAY_MULTIPLIER * forget * rate_ref[...] + add
        a = jnp.exp(log_decay)
        b = us[here, :].astype(F32) * admit * jnp.sqrt(one_minus_exp(2.0 * log_decay, a * a))
        d = 1
        while d < size:
            keep = row_id >= d
            a_before = jnp.where(keep, pltpu.roll(a, d, 0), 1.0)
            b_before = jnp.where(keep, pltpu.roll(b, d, 0), 0.0)
            b = a * b_before + b
            a = a * a_before
            d *= 2
        b = b + a * carry_b
        a = a * carry_a
        hs[here, :] = b
        ca_s[here, :] = a
        return a[size - 1 : size], b[size - 1 : size]

    end_a, end_b = lax.fori_loop(
        0, block // size, scan_step, (jnp.ones((1, chans), F32), jnp.zeros((1, chans), F32))
    )
    ends = ex.shape[1]
    which = lax.broadcasted_iota(jnp.int32, (ends, chans), 0)
    ex[s] = jnp.where(which == 0, end_a, end_b)

    def end_to(other):
        return remote(ex.at[s], ex.at[s], x_send.at[other], x_recv.at[s], (other, t))

    def end_send(other, c):
        end_to(other).start()
        return c

    lax.fori_loop(s + 1, n_sp, end_send, 0)

    def mix_step(j, c):
        here = pl.ds(pl.multiple_of(j * size, size), size)
        cm[here, :] = cm[here, :] + hs[here, :]
        return c

    lax.fori_loop(0, block // size, mix_step, 0)

    def enter(other, state):
        remote(ex.at[other], ex.at[other], x_send.at[other], x_recv.at[other], (other, t)).wait_recv()
        pair = ex[other]
        return pair[0:1] * state + pair[1:2]

    state = lax.fori_loop(0, s, enter, init_ref[...])

    def merge_step(j, c):
        here = pl.ds(pl.multiple_of(j * size, size), size)
        mg[here, :] = (cm[here, :] + ca_s[here, :] * state).astype(BF16)
        return c

    lax.fori_loop(0, block // size, merge_step, 0)

    def rows_of(q):
        return pl.ds(pl.multiple_of(q * rows, 16), rows)

    def merged_to(d):
        q = lax.rem(t + d, n_tp)
        return remote(mg.at[rows_of(q)], mgx.at[t], m_send.at[d], m_recv.at[t], (s, q))

    for d in range(1, n_tp):
        merged_to(d).start()
    mgx[t] = mg[rows_of(t), :]

    rest(wo_at, wo_fwd, wo_recv)

    pieces = oacc.shape[0]
    span = wo_ref.shape[0] // pieces
    for d in range(n_tp):
        q = at(lax.rem(o + d // inner, outer), lax.rem(i + d % inner, inner))
        if d > 0:
            remote(mgx.at[q], mgx.at[q], m_send.at[0], m_recv.at[q], (s, q)).wait_recv()

        def out_step(n, c):
            part = lax.dot_general(
                mgx[q],
                wos[q, pl.ds(pl.multiple_of(n * span, span), span), :],
                (((1,), (1,)), ((), ())),
                preferred_element_type=F32,
            )
            oacc[n] = part if d == 0 else oacc[n] + part
            return c

        lax.fori_loop(0, pieces, out_step, 0)
    for n in range(pieces):
        out_ref[:, n * span : (n + 1) * span] = oacc[n].astype(BF16)

    @pl.when(s + 1 < n_sp)
    def _():
        halo.wait_send()

    def end_wait(other, c):
        end_to(other).wait_send()
        return c

    lax.fori_loop(s + 1, n_sp, end_wait, 0)
    for d in range(1, n_tp):
        merged_to(d).wait_send()
    sent(tok_at, tk_send, tk_fwd, tk_recv)
    sent(wo_at, wo_send, wo_fwd, wo_recv)

    def w_wait(b, c):
        q = b * fast + y

        @pl.when((b <= z) & has_up)
        def _():
            up(q).wait_send()

        @pl.when((b >= z) & has_down)
        def _():
            down(q).wait_send()

        for d in range(1, fast):
            across(q, d).wait_send()
        return c

    lax.fori_loop(0, slow, w_wait, 0)


def layer(
    n_sp, n_tp,
    tokens, gain, w_gate, w_value, w_recur, conv_f, rec_f, g_reset, g_admit, rate, head_add, init, w_out,
):
    rows, model = tokens.shape
    kb, chans = w_gate.shape
    block = rows * n_tp
    fast = 2 if n_sp % 2 == 0 else 1
    while n_sp // fast > 8:
        fast *= 2
    inner = 2 if n_tp % 2 == 0 else 1
    slow, outer = n_sp // fast, n_tp // inner
    heads = g_reset.shape[0]
    pieces = 4
    dma = pltpu.SemaphoreType.DMA
    vmem = pl.BlockSpec(memory_space=pltpu.VMEM)
    anywhere = pl.BlockSpec(memory_space=pl.ANY)
    return pl.pallas_call(
        functools.partial(kernel, n_sp, n_tp, fast, inner),
        out_shape=jax.ShapeDtypeStruct((rows, w_out.shape[0]), BF16),
        in_specs=[anywhere, vmem, anywhere, anywhere, anywhere] + [vmem] * 7 + [anywhere],
        out_specs=vmem,
        scratch_shapes=[
            pltpu.VMEM((HALO + block, model), BF16),
            pltpu.VMEM((slow, HALO + block, model // slow), BF16),
            pltpu.VMEM((3, n_sp, kb, chans), BF16),
            pltpu.VMEM((n_tp,) + w_out.shape, BF16),
            pltpu.VMEM((3, HALO + block, chans), F32),
            pltpu.VMEM((block, chans), BF16),
            pltpu.VMEM((block, chans), F32),
            pltpu.VMEM((block, chans), F32),
            pltpu.VMEM((block, chans), F32),
            pltpu.VMEM((heads, block, 128), F32),
            pltpu.VMEM((n_sp, 8, chans), F32),
            pltpu.VMEM((block, chans), BF16),
            pltpu.VMEM((n_tp, rows, chans), BF16),
            pltpu.VMEM((pieces, rows, w_out.shape[0] // pieces), F32),
            dma((5,)),
            dma((n_sp,)), dma((n_sp,)), dma((n_sp,)), dma((n_sp, fast)),
            dma((n_tp,)), dma((outer,)), dma((outer, inner)),
            dma((n_tp,)), dma((outer,)), dma((outer, inner)),
            dma((2,)), dma((n_sp,)), dma((n_sp,)), dma((n_tp,)), dma((n_tp,)),
        ],
        compiler_params=pltpu.CompilerParams(
            collective_id=0, has_side_effects=True, vmem_limit_bytes=56 * 1024 * 1024
        ),
    )(
        tokens, gain[None, :], w_gate, w_value, w_recur, conv_f, rec_f, g_reset, g_admit,
        rate[None, :], head_add, init[None, :], w_out,
    )


def solution(mesh):
    placed = (
        P(("sp", "tp"), None),
        P(),
        P("sp", "tp"),
        P("sp", "tp"),
        P("sp", "tp"),
        P(None, "tp"),
        P(None, "tp"),
        P("tp", None, None),
        P("tp", None, None),
        P("tp"),
        P("tp", "sp"),
        P("tp"),
        P(None, "tp"),
    )
    return jax.shard_map(
        functools.partial(layer, mesh.shape["sp"], mesh.shape["tp"]),
        mesh=mesh,
        in_specs=placed,
        out_specs=P(("sp", "tp"), None),
        check_vma=False,
    )
```

time: 283 us -> 96.4 us (0.34)
  waiting for transfers between devices: 148 us -> 0 us
  Pallas kernels: 0 us -> 92.4 us
  blocking collectives: 40.8 us -> 0 us
  local copies, waits for them, and re-layouts: 33.3 us -> 3.06 us
  other arithmetic: 17.9 us -> 0 us
  matrix products: 16.4 us -> 0 us
  between operations: 14 us -> 0.01 us
  starting transfers between devices: 10 us -> 0 us
    all_gather x4 -> x0, waiting for transfers between devices: 108 us -> none  [the longest x1 48 us: shards(): lax.all_gather(value_input_weight, 'sp', axis=0, tiled=True)]
    pallas_call x0 -> x1, Pallas kernels: none -> 92.4 us  [layer(): pl.pallas_call(functools.partial(kernel, n_sp, n_tp, fast, inner), out_sh...]
    all_gather x2 -> x0, blocking collectives: 40.8 us -> none  [the longest x1 20.5 us: shards(): lax.all_gather(block_end[None, :], 'sp', axis=0, tiled=True)]
    reduce_scatter x1 -> x0, waiting for transfers between devices: 38.2 us -> none  [shards(): lax.psum_scatter(lax.dot_general(merged, output_matrix, contract, preferr...]
    dot_general x5 -> x0, matrix products: 16.4 us -> none  [the longest x1 6.71 us: shards(): lax.dot_general(merged, output_matrix, contract, preferred_element_type=j...]
    slice x58 -> x0, local copies, waits for them, and re-layouts: 15.2 us -> none  [the longest x56 15.2 us: shards(): lax.associative_scan(linear_step, (decay_step, drive_term), axis=0)]
    pad x30 -> x0, local copies, waits for them, and re-layouts: 10.8 us -> none  [shards(): lax.associative_scan(linear_step, (decay_step, drive_term), axis=0)]
    ppermute x2 -> x0, starting transfers between devices: 9.81 us -> none  [shifted(): lax.ppermute(value, axis, [(source, source + steps) for source in range(f...]
  transfers between devices with their start and end apart: 7 -> 0, of which waited for: 4 -> 0; matrix products, arithmetic and copies ran while one was open for 20% -> 0% of each run, Pallas kernels for 0% -> 0%
where the time goes in v1:
time: 96.4 us; the launch traced here: 95.5 us
  Pallas kernels  92.4 us (96%)
  local copies, waits for them, and re-layouts  3.06 us (3%)
    pallas_call x1, Pallas kernels, layer(): pl.pallas_call(functools.partial(kernel, n_sp, n_tp, fast, inner), out_sh...  92.4 us

profile of v1, /device:TPU:5, one launch (start us, length us, event | category | flops | bytes accessed | tf_op | source)
XLA Modules:
  0.0 95.5 jit_solution(2826632747436654212)
XLA Ops:
  0.0 1.3 %broadcast_in_dim.9.gain_ref = bf16[1,2048]{1,0:T(2,128)(2,1)} reshape(bf16[2048]{0:T(1024)(128)(2,1)} %param.14) | data formatting | bytes 8192 | tf_op jit(solution)/shard_map/broadcast_in_dim | solution.py:462
  1.3 92.4 %shard_map.127 = bf16[96,2048]{1,0:T(8,128)(2,1)} custom-call(bf16[96,2048]{1,0:T(8,128)(2,1)} %tok_ref.1, bf16[1,2048]{1,0:T(2,128)(2,1)} %broadcast_in_dim.9.gain_ref, bf16[256,512]{1,0:T(8,128)(2,1)} %gate_ref.1, bf16[256,512]{1,0:T(8,128)(2,1)} %value_ref.1, bf16[256,512]{1,0:T(8,128)(2,1)} %recur_ref.1, bf16[3,512]{1,0:T(4,128)(2,1)} %cf_ref.1, ...), custom_call_target="tpu_custom_call" | custom-call | tf_op jit(solution)/shard_map/pallas_call | solution.py:432
  93.7 1.8 %copy.15 = bf16[96,2048]{1,0:T(8,128)(2,1)} copy(bf16[96,2048]{1,0:T(8,128)(2,1)} %shard_map.127) | data formatting | bytes 786432

commit v2 on v1

--- a/solution.py
+++ b/solution.py
@@ -38,8 +38,8 @@
     tok_ref, gain_ref, gate_ref, value_ref, recur_ref, cf_ref, rf_ref, gr_ref, gi_ref,
     rate_ref, hl_ref, init_ref, wo_ref,
     out_ref,
-    tokx, nrm, wgt, wos, acc, us, cm, hs, ca_s, hlb, ex, mg, mgx, oacc,
-    loc_sem, w_recv, up_send, dn_send, y_send,
+    tokx, nrm, wgt, wos, acc, us, hs, ca_s, hlb, ex, mg, mgx, oacc,
+    loc_sem, w_recv, up_send, dn_send, y_send, b_recv, b_send,
     tk_recv, tk_send, tk_fwd, wo_recv, wo_send, wo_fwd,
     halo_sem, x_send, x_recv, m_send, m_recv,
 ):
@@ -57,7 +57,7 @@
 
     local = [
         pltpu.make_async_copy(ref, wgt.at[p, s], loc_sem.at[p])
-        for p, ref in enumerate((gate_ref, value_ref, recur_ref))
+        for p, ref in enumerate((recur_ref, value_ref, gate_ref))
     ]
     local.append(pltpu.make_async_copy(tok_ref, tok_at(t), loc_sem.at[3]))
     local.append(pltpu.make_async_copy(wo_ref, wos.at[t], loc_sem.at[4]))
@@ -80,38 +80,63 @@
         copy.wait()
     pl.semaphore_wait(barrier, n_sp + n_tp - 2)
 
-    def slab(q):
-        return wgt.at[:, q]
-
-    def up(q):
-        return remote(slab(q), slab(q), up_send.at[q], w_recv.at[q], (lax.min(s + fast, n_sp - 1), t))
-
-    def down(q):
-        return remote(slab(q), slab(q), dn_send.at[q], w_recv.at[q], (lax.max(s - fast, 0), t))
-
-    def across(q, d):
+    parts = ((0, 1), (1, 2))
+    balance = fast == 2 and slow >= 4
+    half = wgt.shape[2] // 2
+
+    def slab(ph, q, piece=None):
+        first, count = parts[ph]
+        if piece is None:
+            return wgt.at[pl.ds(first, count), q]
+        return wgt.at[pl.ds(first, count), q, pl.ds(piece * half, half)]
+
+    above, below = lax.min(s + fast, n_sp - 1), lax.max(s - fast, 0)
+
+    def up(ph, q):
+        return remote(slab(ph, q), slab(ph, q), up_send.at[ph, q], w_recv.at[ph, q], (above, t))
+
+    def down(ph, q):
+        return remote(slab(ph, q), slab(ph, q), dn_send.at[ph, q], w_recv.at[ph, q], (below, t))
+
+    def across(ph, q, d, piece=None):
+        view = slab(ph, q, piece)
         return remote(
-            slab(q), slab(q), y_send.at[q, d - 1], w_recv.at[q], (z * fast + lax.rem(y + d, fast), t)
+            view, view, y_send.at[ph, lax.div(q, fast), d - 1], w_recv.at[ph, q], (z * fast + lax.rem(y + d, fast), t)
         )
 
-    def arrived(q):
-        across(q, 1).wait_recv()
-
-    def send_across(q):
+    def late(ph, q, where):
+        view = slab(ph, q, 1)
+        return remote(view, view, b_send.at[ph], b_recv.at[ph], (where, t))
+
+    def arrived(ph, q):
+        across(ph, q, 1).wait_recv()
+
+    def send_across(ph, q):
         for d in range(1, fast):
-            across(q, d).start()
+            across(ph, q, d).start()
+
+    def pass_across(ph, q, k, at_end):
+        if balance and k == 1:
+            pl.when(jnp.logical_not(at_end))(lambda: send_across(ph, q))
+        elif balance and k == slow - 1:
+            across(ph, q, 1, 0).start()
+        else:
+            send_across(ph, q)
 
     has_up, has_down = z + 1 < slow, z >= 1
 
-    @pl.when(has_up)
-    def _():
-        up(s).start()
-
-    @pl.when(has_down)
-    def _():
-        down(s).start()
-
-    send_across(s)
+    def begin(ph):
+        @pl.when(has_up)
+        def _():
+            up(ph, s).start()
+
+        @pl.when(has_down)
+        def _():
+            down(ph, s).start()
+
+        send_across(ph, s)
+
+    begin(0)
 
     def at(oo, ii):
         return oo * inner + ii
@@ -175,7 +200,7 @@
     def normalize(r0):
         x = tokx[pl.ds(r0, HALO), :].astype(F32)
         inv = lax.rsqrt(jnp.mean(x * x, axis=1, keepdims=True) + NORM_EPS)
-        n = (x * inv * gain_ref[...].astype(F32)).astype(BF16)
+        n = (x * inv * gain_ref[...].astype(F32)[None, :]).astype(BF16)
         for b in range(slow):
             nrm[b, pl.ds(r0, HALO), :] = n[:, b * kz : (b + 1) * kz]
 
@@ -195,91 +220,119 @@
 
     normalize(0)
 
-    def multiply(b, first):
-        for d in range(1, fast):
-            arrived(b * fast + lax.rem(y + d, fast))
+    other = z * fast + lax.rem(y + 1, fast)
+
+    def multiply(ph, b, k):
+        ends = balance and k == slow - 1
+        if ends:
+            q = b * fast + lax.rem(y + 1, fast)
+            across(ph, q, 1, 0).wait_recv()
+            late(ph, q, s).wait_recv()
+        else:
+            for d in range(1, fast):
+                arrived(ph, b * fast + lax.rem(y + d, fast))
+        if balance and k == 0:
+            @pl.when(z == 0)
+            def _():
+                up(ph, other).start()
+
+            @pl.when(z == slow - 1)
+            def _():
+                down(ph, other).start()
+
+        if balance and k == slow - 2:
+            q = b * fast + lax.rem(y + 1, fast)
+
+            @pl.when((z == slow - 2) & (b == 0))
+            def _():
+                late(ph, q, above).start()
+
+            @pl.when((z == 1) & (b == slow - 1))
+            def _():
+                late(ph, q, below).start()
 
         def step(p, c):
             w = wgt[p, pl.ds(b * fast, fast)].reshape(kz, chans)
             part = jnp.dot(nrm[b], w, preferred_element_type=F32)
-            if first:
+            if k == 0:
                 acc[p] = part
             else:
                 acc[p] = acc[p] + part
             return c
 
-        lax.fori_loop(0, 3, step, 0)
-
-    def multiply_step(k):
+        first, count = parts[ph]
+        lax.fori_loop(first, first + count, step, 0)
+
+    def multiply_step(ph, k):
         if k == 0:
-            multiply(z, True)
+            multiply(ph, z, 0)
             return
 
         @pl.when(z >= k)
         def _():
-            multiply(z - k, False)
+            multiply(ph, z - k, k)
 
         @pl.when(z + k < slow)
         def _():
-            multiply(z + k, False)
-
-    for k in range(1, slow):
+            multiply(ph, z + k, k)
+
+    def forward(ph, k):
         @pl.when(z >= k)
         def _():
             q = s - k * fast
-            arrived(q)
+            arrived(ph, q)
 
             @pl.when(has_up)
             def _():
-                up(q).start()
-
-            send_across(q)
+                up(ph, q).start()
+
+            pass_across(ph, q, k, z == k)
 
         @pl.when(z + k < slow)
         def _():
             q = s + k * fast
-            arrived(q)
+            arrived(ph, q)
 
             @pl.when(has_down)
             def _():
-                down(q).start()
-
-            send_across(q)
-
-        multiply_step(k - 1)
-    multiply_step(slow - 1)
-
-    pass_on(wo_at, wo_fwd, wo_recv, wo_send)
+                down(ph, q).start()
+
+            pass_across(ph, q, k, z + k == slow - 1)
+
+    for k in range(1, slow):
+        forward(0, k)
+        multiply_step(0, k - 1)
+    begin(1)
+    multiply_step(0, slow - 1)
 
     size = 32
-    v_taps, r_taps = cf_ref.shape[0], rf_ref.shape[0]
-
-    def conv_step(j, c):
+
+    def window(p, r0):
+        return acc[p, pl.ds(pl.multiple_of(r0 + HALO - 8, 8), size + 8), :].astype(BF16).astype(F32)
+
+    def taps(x, ref):
+        n = ref.shape[0]
+        first = 8 - (n - 1)
+        total = ref[0:1, :].astype(F32) * x[first : first + size]
+        for k in range(1, n):
+            total = total + ref[k : k + 1, :].astype(F32) * x[first + k : first + k + size]
+        return total
+
+    def recur_step(j, c):
         r0 = pl.multiple_of(j * size, size)
-
-        def window(p):
-            return acc[p, pl.ds(pl.multiple_of(r0 + HALO - 8, 8), size + 8), :].astype(BF16).astype(F32)
-
-        def taps(x, ref):
-            n = ref.shape[0]
-            first = 8 - (n - 1)
-            total = ref[0:1, :].astype(F32) * x[first : first + size]
-            for k in range(1, n):
-                total = total + ref[k : k + 1, :].astype(F32) * x[first + k : first + k + size]
-            return total
-
-        us[pl.ds(r0, size), :] = taps(window(2), rf_ref).astype(BF16)
-        cm[pl.ds(r0, size), :] = window(0)[8:] * taps(window(1), cf_ref)
-        return c
-
-    lax.fori_loop(0, block // size, conv_step, 0)
+        us[pl.ds(r0, size), :] = taps(window(0, r0), rf_ref).astype(BF16)
+        return c
+
+    lax.fori_loop(0, block // size, recur_step, 0)
 
     heads, width = gr_ref.shape[0], gr_ref.shape[1]
     for h in range(heads):
         cols = pl.ds(h * width, width)
         u = us[:, cols]
-        acc[0, pl.ds(0, block), cols] = jnp.dot(u, gr_ref[h], preferred_element_type=F32)
-        acc[1, pl.ds(0, block), cols] = jnp.dot(u, gi_ref[h], preferred_element_type=F32)
+        ca_s[:, cols] = jnp.dot(u, gr_ref[h], preferred_element_type=F32)
+        hs[:, cols] = jnp.dot(u, gi_ref[h], preferred_element_type=F32)
+    forward(1, 1)
+    multiply_step(1, 0)
 
     row_id = lax.broadcasted_iota(jnp.int32, (size, chans), 0)
 
@@ -287,8 +340,8 @@
         carry_a, carry_b = carry
         r0 = pl.multiple_of(j * size, size)
         here = pl.ds(r0, size)
-        forget = 1.0 / (1.0 + jnp.exp(-acc[0, here, :]))
-        admit = 1.0 / (1.0 + jnp.exp(-acc[1, here, :]))
+        forget = 1.0 / (1.0 + jnp.exp(-ca_s[here, :]))
+        admit = 1.0 / (1.0 + jnp.exp(-hs[here, :]))
         add = jnp.concatenate(
             [hlb[h, here, :] for h in range(heads) for _ in range(width // lanes)], axis=1
         )
@@ -316,32 +369,40 @@
     which = lax.broadcasted_iota(jnp.int32, (ends, chans), 0)
     ex[s] = jnp.where(which == 0, end_a, end_b)
 
-    def end_to(other):
-        return remote(ex.at[s], ex.at[s], x_send.at[other], x_recv.at[s], (other, t))
-
-    def end_send(other, c):
-        end_to(other).start()
+    def end_to(later):
+        return remote(ex.at[s], ex.at[s], x_send.at[later], x_recv.at[s], (later, t))
+
+    def end_send(later, c):
+        end_to(later).start()
         return c
 
     lax.fori_loop(s + 1, n_sp, end_send, 0)
+    for k in range(2, slow):
+        forward(1, k)
+        multiply_step(1, k - 1)
+
+    def enter(prior, state):
+        remote(ex.at[prior], ex.at[prior], x_send.at[prior], x_recv.at[prior], (prior, t)).wait_recv()
+        pair = ex[prior]
+        return pair[0:1] * state + pair[1:2]
+
+    state = lax.fori_loop(0, s, enter, init_ref[...])
 
     def mix_step(j, c):
         here = pl.ds(pl.multiple_of(j * size, size), size)
-        cm[here, :] = cm[here, :] + hs[here, :]
+        hs[here, :] = hs[here, :] + ca_s[here, :] * state
         return c
 
     lax.fori_loop(0, block // size, mix_step, 0)
-
-    def enter(other, state):
-        remote(ex.at[other], ex.at[other], x_send.at[other], x_recv.at[other], (other, t)).wait_recv()
-        pair = ex[other]
-        return pair[0:1] * state + pair[1:2]
-
-    state = lax.fori_loop(0, s, enter, init_ref[...])
+    multiply_step(1, slow - 1)
+
+    pass_on(wo_at, wo_fwd, wo_recv, wo_send)
 
     def merge_step(j, c):
-        here = pl.ds(pl.multiple_of(j * size, size), size)
-        mg[here, :] = (cm[here, :] + ca_s[here, :] * state).astype(BF16)
+        r0 = pl.multiple_of(j * size, size)
+        here = pl.ds(r0, size)
+        conv_mix = window(2, r0)[8:] * taps(window(1, r0), cf_ref)
+        mg[here, :] = (conv_mix + hs[here, :]).astype(BF16)
         return c
 
     lax.fori_loop(0, block // size, merge_step, 0)
@@ -384,8 +445,8 @@
     def _():
         halo.wait_send()
 
-    def end_wait(other, c):
-        end_to(other).wait_send()
+    def end_wait(later, c):
+        end_to(later).wait_send()
         return c
 
     lax.fori_loop(s + 1, n_sp, end_wait, 0)
@@ -396,20 +457,45 @@
 
     def w_wait(b, c):
         q = b * fast + y
-
-        @pl.when((b <= z) & has_up)
-        def _():
-            up(q).wait_send()
-
-        @pl.when((b >= z) & has_down)
-        def _():
-            down(q).wait_send()
-
-        for d in range(1, fast):
-            across(q, d).wait_send()
+        for ph in range(len(parts)):
+            @pl.when((b <= z) & has_up)
+            def _():
+                up(ph, q).wait_send()
+
+            @pl.when((b >= z) & has_down)
+            def _():
+                down(ph, q).wait_send()
+
+            if not balance:
+                for d in range(1, fast):
+                    across(ph, q, d).wait_send()
+                continue
+            skip = ((z == 1) & (b == 0)) | ((z == slow - 2) & (b == slow - 1))
+            part = ((z == slow - 1) & (b == 0)) | ((z == 0) & (b == slow - 1))
+
+            @pl.when(part)
+            def _():
+                across(ph, q, 1, 0).wait_send()
+
+            @pl.when(jnp.logical_not(skip | part))
+            def _():
+                across(ph, q, 1).wait_send()
         return c
 
     lax.fori_loop(0, slow, w_wait, 0)
+    if balance:
+        for ph in range(len(parts)):
+            @pl.when(z == 0)
+            def _():
+                up(ph, other).wait_send()
+
+            @pl.when(z == slow - 1)
+            def _():
+                down(ph, other).wait_send()
+
+            @pl.when((z == 1) | (z == slow - 2))
+            def _():
+                late(ph, s, s).wait_send()
 
 
 def layer(
@@ -443,14 +529,13 @@
             pltpu.VMEM((block, chans), BF16),
             pltpu.VMEM((block, chans), F32),
             pltpu.VMEM((block, chans), F32),
-            pltpu.VMEM((block, chans), F32),
             pltpu.VMEM((heads, block, 128), F32),
             pltpu.VMEM((n_sp, 8, chans), F32),
             pltpu.VMEM((block, chans), BF16),
             pltpu.VMEM((n_tp, rows, chans), BF16),
             pltpu.VMEM((pieces, rows, w_out.shape[0] // pieces), F32),
             dma((5,)),
-            dma((n_sp,)), dma((n_sp,)), dma((n_sp,)), dma((n_sp, fast)),
+            dma((2, n_sp)), dma((2, n_sp)), dma((2, n_sp)), dma((2, slow, fast)), dma((2,)), dma((2,)),
             dma((n_tp,)), dma((outer,)), dma((outer, inner)),
             dma((n_tp,)), dma((outer,)), dma((outer, inner)),
             dma((2,)), dma((n_sp,)), dma((n_sp,)), dma((n_tp,)), dma((n_tp,)),
@@ -459,7 +544,7 @@
             collective_id=0, has_side_effects=True, vmem_limit_bytes=56 * 1024 * 1024
         ),
     )(
-        tokens, gain[None, :], w_gate, w_value, w_recur, conv_f, rec_f, g_reset, g_admit,
+        tokens, gain, w_gate, w_value, w_recur, conv_f, rec_f, g_reset, g_admit,
         rate[None, :], head_add, init[None, :], w_out,
     )
 

time: 96.4 us -> 95.1 us (0.987)
  local copies, waits for them, and re-layouts: 3.06 us -> 1.77 us
    broadcast_in_dim x1 -> x0, local copies, waits for them, and re-layouts: 1.29 us -> none  [layer(): gain[None, :]]
where the time goes in v2:
time: 95.1 us; the launch traced here: 94.1 us
  Pallas kernels  92.3 us (97%)
  local copies, waits for them, and re-layouts  1.77 us (2%)
    pallas_call x1, Pallas kernels, layer(): pl.pallas_call(functools.partial(kernel, n_sp, n_tp, fast, inner), out_sh...  92.3 us

profile of v2, /device:TPU:5, one launch (start us, length us, event | category | flops | bytes accessed | tf_op | source)
XLA Modules:
  0.0 94.1 jit_solution(9959962020531520087)
XLA Ops:
  0.0 92.3 %shard_map.127 = bf16[96,2048]{1,0:T(8,128)(2,1)} custom-call(bf16[96,2048]{1,0:T(8,128)(2,1)} %tok_ref.1, bf16[2048]{0:T(1024)(128)(2,1)} %gain_ref.1, bf16[256,512]{1,0:T(8,128)(2,1)} %gate_ref.1, bf16[256,512]{1,0:T(8,128)(2,1)} %value_ref.1, bf16[256,512]{1,0:T(8,128)(2,1)} %recur_ref.1, bf16[3,512]{1,0:T(4,128)(2,1)} %cf_ref.1, bf16[4,512]{1,0:T(4,128)(2,1)} %rf_ref.1, ...), custom_call_target="tpu_custom_call" | custom-call | tf_op jit(solution)/shard_map/pallas_call | solution.py:518
  92.3 1.8 %copy.15 = bf16[96,2048]{1,0:T(8,128)(2,1)} copy(bf16[96,2048]{1,0:T(8,128)(2,1)} %shard_map.127) | data formatting | bytes 786432

commit v3 on v2

--- a/solution.py
+++ b/solution.py
@@ -80,7 +80,7 @@
         copy.wait()
     pl.semaphore_wait(barrier, n_sp + n_tp - 2)
 
-    parts = ((0, 1), (1, 2))
+    parts = ((0, 1), (1, 1), (2, 1))
     balance = fast == 2 and slow >= 4
     half = wgt.shape[2] // 2
 
@@ -137,6 +137,7 @@
         send_across(ph, s)
 
     begin(0)
+    begin(1)
 
     def at(oo, ii):
         return oo * inner + ii
@@ -185,44 +186,9 @@
     for h in range(hl_ref.shape[0]):
         hlb[h] = jnp.broadcast_to(hl_ref[h : h + 1, :], (lanes, block)).T
 
-    pass_on(tok_at, tk_fwd, tk_recv, tk_send)
-    rest(tok_at, tk_fwd, tk_recv)
-
-    halo = remote(
-        tokx.at[pl.ds(block, HALO)], tokx.at[pl.ds(0, HALO)],
-        halo_sem.at[0], halo_sem.at[1], (lax.min(s + 1, n_sp - 1), t),
-    )
-
-    @pl.when(s + 1 < n_sp)
-    def _():
-        halo.start()
-
-    def normalize(r0):
-        x = tokx[pl.ds(r0, HALO), :].astype(F32)
-        inv = lax.rsqrt(jnp.mean(x * x, axis=1, keepdims=True) + NORM_EPS)
-        n = (x * inv * gain_ref[...].astype(F32)[None, :]).astype(BF16)
-        for b in range(slow):
-            nrm[b, pl.ds(r0, HALO), :] = n[:, b * kz : (b + 1) * kz]
-
-    def norm_step(r, c):
-        normalize(pl.multiple_of(r * HALO, HALO))
-        return c
-
-    lax.fori_loop(1, block // HALO + 1, norm_step, 0)
-
-    @pl.when(s == 0)
-    def _():
-        tokx[pl.ds(0, HALO), :] = jnp.zeros((HALO, tokx.shape[1]), BF16)
-
-    @pl.when(s > 0)
-    def _():
-        halo.wait_recv()
-
-    normalize(0)
-
     other = z * fast + lax.rem(y + 1, fast)
 
-    def multiply(ph, b, k):
+    def collect_block(ph, b, k):
         ends = balance and k == slow - 1
         if ends:
             q = b * fast + lax.rem(y + 1, fast)
@@ -251,6 +217,7 @@
             def _():
                 late(ph, q, below).start()
 
+    def dots_block(ph, b, k):
         def step(p, c):
             w = wgt[p, pl.ds(b * fast, fast)].reshape(kz, chans)
             part = jnp.dot(nrm[b], w, preferred_element_type=F32)
@@ -263,18 +230,24 @@
         first, count = parts[ph]
         lax.fori_loop(first, first + count, step, 0)
 
-    def multiply_step(ph, k):
+    def at_distance(act, ph, k):
         if k == 0:
-            multiply(ph, z, 0)
+            act(ph, z, 0)
             return
 
         @pl.when(z >= k)
         def _():
-            multiply(ph, z - k, k)
+            act(ph, z - k, k)
 
         @pl.when(z + k < slow)
         def _():
-            multiply(ph, z + k, k)
+            act(ph, z + k, k)
+
+    def collect(ph, k):
+        at_distance(collect_block, ph, k)
+
+    def dots(ph, k):
+        at_distance(dots_block, ph, k)
 
     def forward(ph, k):
         @pl.when(z >= k)
@@ -299,11 +272,66 @@
 
             pass_across(ph, q, k, z + k == slow - 1)
 
-    for k in range(1, slow):
+    forward(0, 1)
+    collect(0, 0)
+    begin(2)
+
+    pass_on(tok_at, tk_fwd, tk_recv, tk_send)
+    rest(tok_at, tk_fwd, tk_recv)
+
+    halo = remote(
+        tokx.at[pl.ds(block, HALO)], tokx.at[pl.ds(0, HALO)],
+        halo_sem.at[0], halo_sem.at[1], (lax.min(s + 1, n_sp - 1), t),
+    )
+
+    @pl.when(s + 1 < n_sp)
+    def _():
+        halo.start()
+
+    def normalize(r0):
+        x = tokx[pl.ds(r0, HALO), :].astype(F32)
+        inv = lax.rsqrt(jnp.mean(x * x, axis=1, keepdims=True) + NORM_EPS)
+        n = (x * inv * gain_ref[...].astype(F32)[None, :]).astype(BF16)
+        for b in range(slow):
+            nrm[b, pl.ds(r0, HALO), :] = n[:, b * kz : (b + 1) * kz]
+
+    def norm_step(r, c):
+        normalize(pl.multiple_of(r * HALO, HALO))
+        return c
+
+    lax.fori_loop(1, block // HALO + 1, norm_step, 0)
+
+    forward(0, 2)
+    forward(1, 1)
+    collect(1, 0)
+    collect(0, 1)
+    for k in range(3, slow):
         forward(0, k)
-        multiply_step(0, k - 1)
-    begin(1)
-    multiply_step(0, slow - 1)
+        forward(1, k - 1)
+        forward(2, k - 2)
+        if k == 3:
+            collect(2, 0)
+        collect(0, k - 1)
+        if k < slow - 1:
+            collect(1, k - 2)
+            collect(2, k - 3) if k > 3 else None
+
+    @pl.when(s == 0)
+    def _():
+        tokx[pl.ds(0, HALO), :] = jnp.zeros((HALO, tokx.shape[1]), BF16)
+
+    @pl.when(s > 0)
+    def _():
+        halo.wait_recv()
+
+    normalize(0)
+    for k in range(slow - 1):
+        dots(0, k)
+    collect(1, slow - 3)
+    forward(1, slow - 1)
+    forward(2, slow - 2)
+    collect(0, slow - 1)
+    dots(0, slow - 1)
 
     size = 32
 
@@ -331,8 +359,11 @@
         u = us[:, cols]
         ca_s[:, cols] = jnp.dot(u, gr_ref[h], preferred_element_type=F32)
         hs[:, cols] = jnp.dot(u, gi_ref[h], preferred_element_type=F32)
-    forward(1, 1)
-    multiply_step(1, 0)
+    collect(1, slow - 2)
+    if slow > 4:
+        collect(2, slow - 4)
+    collect(2, slow - 3)
+    forward(2, slow - 1)
 
     row_id = lax.broadcasted_iota(jnp.int32, (size, chans), 0)
 
@@ -377,9 +408,11 @@
         return c
 
     lax.fori_loop(s + 1, n_sp, end_send, 0)
-    for k in range(2, slow):
-        forward(1, k)
-        multiply_step(1, k - 1)
+    for k in range(slow - 1):
+        dots(1, k)
+    collect(1, slow - 1)
+    dots(1, slow - 1)
+    collect(2, slow - 2)
 
     def enter(prior, state):
         remote(ex.at[prior], ex.at[prior], x_send.at[prior], x_recv.at[prior], (prior, t)).wait_recv()
@@ -394,7 +427,10 @@
         return c
 
     lax.fori_loop(0, block // size, mix_step, 0)
-    multiply_step(1, slow - 1)
+    for k in range(slow - 1):
+        dots(2, k)
+    collect(2, slow - 1)
+    dots(2, slow - 1)
 
     pass_on(wo_at, wo_fwd, wo_recv, wo_send)
 
@@ -535,7 +571,7 @@
             pltpu.VMEM((n_tp, rows, chans), BF16),
             pltpu.VMEM((pieces, rows, w_out.shape[0] // pieces), F32),
             dma((5,)),
-            dma((2, n_sp)), dma((2, n_sp)), dma((2, n_sp)), dma((2, slow, fast)), dma((2,)), dma((2,)),
+            dma((3, n_sp)), dma((3, n_sp)), dma((3, n_sp)), dma((3, slow, fast)), dma((3,)), dma((3,)),
             dma((n_tp,)), dma((outer,)), dma((outer, inner)),
             dma((n_tp,)), dma((outer,)), dma((outer, inner)),
             dma((2,)), dma((n_sp,)), dma((n_sp,)), dma((n_tp,)), dma((n_tp,)),

time: 95.1 us -> 82.3 us (0.87)
  Pallas kernels: 92.3 us -> 80.3 us
    pallas_call x1, Pallas kernels: 92.3 us -> 80.3 us  [layer(): pl.pallas_call(functools.partial(kernel, n_sp, n_tp, fast, inner), out_sh...]
where the time goes in v3:
time: 82.3 us; the launch traced here: 82.1 us
  Pallas kernels  80.3 us (98%)
  local copies, waits for them, and re-layouts  1.77 us (2%)
    pallas_call x1, Pallas kernels, layer(): pl.pallas_call(functools.partial(kernel, n_sp, n_tp, fast, inner), out_sh...  80.3 us
    unnamed x1, local copies, waits for them, and re-layouts  1.77 us

profile of v3, /device:TPU:5, one launch (start us, length us, event | category | flops | bytes accessed | tf_op | source)
XLA Modules:
  0.0 82.1 jit_solution(7936611206456720702)
XLA Ops:
  0.0 80.3 %shard_map.127 = bf16[96,2048]{1,0:T(8,128)(2,1)} custom-call(bf16[96,2048]{1,0:T(8,128)(2,1)} %tok_ref.1, bf16[2048]{0:T(1024)(128)(2,1)} %gain_ref.1, bf16[256,512]{1,0:T(8,128)(2,1)} %gate_ref.1, bf16[256,512]{1,0:T(8,128)(2,1)} %value_ref.1, bf16[256,512]{1,0:T(8,128)(2,1)} %recur_ref.1, bf16[3,512]{1,0:T(4,128)(2,1)} %cf_ref.1, bf16[4,512]{1,0:T(4,128)(2,1)} %rf_ref.1, ...), custom_call_target="tpu_custom_call" | custom-call | tf_op jit(solution)/shard_map/pallas_call | solution.py:554
  80.4 1.8 %copy.15 = bf16[96,2048]{1,0:T(8,128)(2,1)} copy(bf16[96,2048]{1,0:T(8,128)(2,1)} %shard_map.127) | data formatting | bytes 786432
